TPU v7x, 512 devices: a whole 4x8x8 slice. The times are simulated.
512 devices in a mesh: sp: 32 (over z, x), tp: 16 (over y, core).
Axes of the slice: x: 4, y: 8, z: 8, core: 2. Of those that a mesh axis runs over, the one named last changes fastest.
Arguments:
- resid: bfloat16 [4096, 2048], P('sp'), may hold values from -6 to 6
- norm_gain: float32 [2048], replicated, may hold values from 0.1 to 1.9
- cotangent: bfloat16 [4096, 2048], P('sp'), may hold values from -6 to 6
- route_ids: int32 [4096, 2], P('sp'), may hold values from 0 to 31, all different within a row; in each aligned block of 128 rows (0 to 127, 128 to 255, ...) at most 12 rows name the same one
- route_weight: float32 [4096, 2], P('sp'), may hold values from 0.25 to 2.25
- expert_gate: bfloat16 [32, 2048, 2048], P('sp', None, 'tp'), may hold values from -0.125 to 0.125
- expert_up: bfloat16 [32, 2048, 2048], P('sp', None, 'tp'), may hold values from -0.125 to 0.125
- expert_down: bfloat16 [32, 2048, 2048], P('sp', 'tp'), may hold values from -0.125 to 0.125
- out_proj: bfloat16 [2048, 4096], P('sp', 'tp'), may hold values from -0.09375 to 0.09375
- mixed: bfloat16 [4096, 4096], P('sp', 'tp'), may hold values from -6 to 6
- query: bfloat16 [4096, 2048], P('sp', 'tp'), may hold values from -6 to 6
- key: bfloat16 [4096, 2048], P('sp', 'tp'), may hold values from -1.5 to 1.5
- value: bfloat16 [4096, 4096], P('sp', 'tp'), may hold values from -6 to 6
- log_decay: float32 [4096, 2048], P('sp', 'tp'), may hold values from -1 to 0, as said below
- span_state: float32 [32, 16, 128, 256], P('sp', 'tp'), may hold values from -24 to 24
Outputs:
- grad_expert_gate: bfloat16 [32, 2048, 2048], P('sp', None, 'tp')
- grad_expert_up: bfloat16 [32, 2048, 2048], P('sp', None, 'tp')
- grad_expert_down: bfloat16 [32, 2048, 2048], P('sp', 'tp')
- grad_out_proj: float32 [2048, 4096], P('sp', 'tp')
- grad_query: bfloat16 [4096, 2048], P('sp', 'tp')
- grad_key: bfloat16 [4096, 2048], P('sp', 'tp')
- grad_value: bfloat16 [4096, 4096], P('sp', 'tp')
- grad_log_decay: float32 [4096, 2048], P('sp', 'tp')
Inputs may be any that keep to these rules, and one draw needn't show every extreme that they name: `route_ids`: A row names 2 different experts. Within each aligned block of 128 rows (the rows of one index of sp) no expert is named by more than 12 rows, and in every draw some expert is named by exactly 12 rows of some block. `log_decay`: every entry is zero or negative.
All inputs are finite; a program needn't handle non-finite values.
Results may differ from a plain program's by a relative error of at most 0.023.
Values may be sent and summed in bfloat16 or wider, within the bound.
No kernel may reach another device: no remote copies, remote signals or barrier semaphores. Data moves between devices by JAX's collectives and lax.ppermute only.
A program may use at most 64 MiB of HBM per device.

v0:
```python
import jax
import jax.numpy as jnp
from jax import lax
from jax.sharding import Mesh
from jax.sharding import PartitionSpec as P

KEY_CHANNELS = 128
DV = 256
TOP = 2
BLOCK = 64
SP = ("z", "x")
TP = ("y", "c")
epsilon = 1e-06


def sum_parts(tiles):
    return jnp.sum(tiles.astype(jnp.float32), axis=0)


def later_sum(states, decays, place):
    count = states.shape[0]
    total = jnp.zeros(states.shape[1:], jnp.float32)
    factor = jnp.ones(decays.shape[1:], jnp.float32)
    for k in range(count):
        later = k > place
        total = total + jnp.where(later, factor, 0.0)[:, None] * states[k].astype(jnp.float32)
        factor = jnp.where(later, factor * decays[k], factor)
    return (total, factor)


def to_all(array, axis):
    count = lax.axis_size(axis)
    copies = jnp.broadcast_to(array[None], (count, *array.shape))
    return lax.all_to_all(copies, axis, 0, 0, tiled=True)


def with_decay(state, decay):
    row = jnp.pad(decay[None, :], ((0, 7), (0, DV - KEY_CHANNELS)))
    return jnp.concatenate([state, row], axis=0).astype(jnp.bfloat16)


def split_decay(filled):
    decays = filled[:, KEY_CHANNELS, :KEY_CHANNELS].astype(jnp.float32)
    return (filled[:, :KEY_CHANNELS], decays)


def into_blocks(values):
    return values.reshape(values.shape[0] // BLOCK, BLOCK, values.shape[1])


def span_forward(query_rows, key_rows, value_rows, grad_rows, decay_rows, entry_state):
    query_blk = into_blocks(query_rows)
    key_blk = into_blocks(key_rows)
    value_blk = into_blocks(value_rows)
    grad_blk = into_blocks(grad_rows)
    cumlog = jnp.cumsum(into_blocks(decay_rows), axis=1)
    block_total = cumlog[:, -1, :]
    to_end = jnp.exp(block_total[:, None, :] - cumlog)
    inner_part = jnp.einsum("nsd,nsj->ndj", key_blk * to_end, value_blk)

    def forward_step(carry_state, step_item):
        piece_part, block_sum = step_item
        return (jnp.exp(block_sum)[:, None] * carry_state + piece_part, carry_state)

    end_state, starts = lax.scan(forward_step, entry_state, (inner_part, block_total))
    own_part = jnp.einsum("ntd,ntj->ndj", query_blk * jnp.exp(cumlog), grad_blk)

    def backward_step(carry_state, step_item):
        piece_part, block_sum = step_item
        return (jnp.exp(block_sum)[:, None] * carry_state + piece_part, carry_state)

    start_cot, after_cot = lax.scan(
        backward_step, jnp.zeros_like(entry_state), (own_part, block_total), reverse=True
    )
    span_total = jnp.sum(block_total, axis=0)
    later_log = span_total[None, :] - jnp.cumsum(block_total, axis=0)
    return ((cumlog, starts, after_cot, later_log, end_state), (jnp.exp(span_total), start_cot))


def span_backward(query_rows, key_rows, value_rows, grad_rows, kept_terms, exit_cot):
    cumlog, starts, after_cot, later_log, end_state = kept_terms
    query_blk = into_blocks(query_rows)
    key_blk = into_blocks(key_rows)
    value_blk = into_blocks(value_rows)
    grad_blk = into_blocks(grad_rows)
    exit_cots = after_cot + jnp.exp(later_log)[:, :, None] * exit_cot
    causal = jnp.arange(BLOCK)[:, None] >= jnp.arange(BLOCK)[None, :]
    decays = jnp.exp(
        jnp.where(causal[None, :, :, None], cumlog[:, :, None, :] - cumlog[:, None, :, :], -jnp.inf)
    )
    scores = jnp.einsum("ntd,nsd,ntsd->nts", query_blk, key_blk, decays)
    grad_scores = jnp.einsum("ntj,nsj->nts", grad_blk, value_blk)
    grad_query = jnp.exp(cumlog) * jnp.einsum("ntj,ndj->ntd", grad_blk, starts)
    grad_query = grad_query + jnp.einsum("nts,nsd,ntsd->ntd", grad_scores, key_blk, decays)
    to_end = jnp.exp(cumlog[:, -1:, :] - cumlog)
    grad_key = jnp.einsum("nts,ntd,ntsd->nsd", grad_scores, query_blk, decays)
    grad_key = grad_key + to_end * jnp.einsum("nsj,ndj->nsd", value_blk, exit_cots)
    grad_value = jnp.einsum("nts,ntj->nsj", scores, grad_blk)
    grad_value = grad_value + jnp.einsum("nsd,ndj->nsj", key_blk * to_end, exit_cots)
    length = query_rows.shape[0]
    key_width = query_rows.shape[1]
    per_position = (query_blk * grad_query - key_blk * grad_key).reshape(length, key_width)
    grad_log = (
        jnp.flip(jnp.cumsum(jnp.flip(per_position, 0), 0), 0)
        + jnp.sum(end_state * exit_cot, axis=1)[None, :]
    )
    return (
        grad_query.reshape(length, key_width),
        grad_key.reshape(length, key_width),
        grad_value.reshape(length, value_rows.shape[1]),
        grad_log,
    )


def on_device(
    resid,
    norm_gain,
    cotangent,
    route_ids,
    route_weight,
    expert_gate,
    expert_up,
    expert_down,
    out_proj,
    mixed,
    query,
    key,
    value,
    log_decay,
    span_state,
):
    tokens_here = resid.shape[0]
    model_width = resid.shape[1]
    half = model_width // 2
    sp_count = lax.axis_size(SP)
    y_count = lax.axis_size("y")
    experts = sp_count * expert_gate.shape[0]
    capacity = 3 * tokens_here // experts
    slots = experts * capacity
    core = lax.axis_index("c")
    resid_f = resid.astype(jnp.float32)
    inverse_rms = lax.rsqrt(jnp.mean(resid_f * resid_f, axis=1, keepdims=True) + epsilon)
    unit_rows = resid_f * inverse_rms
    normed = (unit_rows * norm_gain).astype(jnp.bfloat16)
    pair_expert = route_ids.reshape(-1)
    onehot = (pair_expert[:, None] == jnp.arange(experts, dtype=jnp.int32)[None, :]).astype(
        jnp.int32
    )
    slot_rank = jnp.sum((jnp.cumsum(onehot, axis=0) - onehot) * onehot, axis=1)
    slot_of = (pair_expert * capacity + slot_rank).reshape(tokens_here, TOP)
    slot_a, slot_b = (slot_of[:, 0], slot_of[:, 1])
    packed = lax.broadcasted_iota(jnp.int32, (2 * slots, 2 * tokens_here), 0)
    aim_a = jnp.concatenate([2 * slot_a, 2 * slot_a + 1])[None, :]
    aim_b = jnp.concatenate([2 * slot_b, 2 * slot_b + 1])[None, :]
    hit_a, hit_b = (packed == aim_a, packed == aim_b)
    weight_a = jnp.concatenate([route_weight[:, 0]] * 2)[None, :]
    weight_b = jnp.concatenate([route_weight[:, 1]] * 2)[None, :]
    slot_weight = jnp.sum(
        jnp.where(hit_a, weight_a, 0.0) + jnp.where(hit_b, weight_b, 0.0), axis=1, keepdims=True
    )
    scale = jnp.where(core == 0, 1.0, slot_weight)
    chosen = jnp.where(core == 0, normed, cotangent)
    rows_two = jnp.concatenate([chosen[:, :half], chosen[:, half:]], axis=0)
    sent = jnp.dot(
        (hit_a | hit_b).astype(jnp.bfloat16), rows_two, preferred_element_type=jnp.float32
    )
    sent = (sent * scale).astype(jnp.bfloat16).reshape(sp_count, 2 * capacity, half)
    own = lax.all_to_all(sent, SP, 0, 0, tiled=True).reshape(2 * slots, half)
    other = lax.ppermute(own, "c", [(0, 1), (1, 0)])
    rows_in = jnp.where(core == 0, own, other)
    rows_cot = jnp.where(core == 0, other, own)
    gate_w, up_w, down_w = (expert_gate[0], expert_up[0], expert_down[0])
    width = gate_w.shape[1]
    into_w = jnp.concatenate([gate_w[:half], gate_w[half:], up_w[:half], up_w[half:]], axis=1)
    down_two = jnp.concatenate([down_w[:, :half], down_w[:, half:]], axis=0)
    pre = jnp.dot(rows_in, into_w, preferred_element_type=jnp.float32)
    gate_pre = pre[:, :width] + jnp.roll(pre[:, width : 2 * width], -1, axis=0)
    up_pre = pre[:, 2 * width : 3 * width] + jnp.roll(pre[:, 3 * width :], -1, axis=0)
    hid = lax.dot_general(
        rows_cot, down_two, (((1,), (1,)), ((), ())), preferred_element_type=jnp.float32
    )
    grad_hidden = hid[:, :width] + jnp.roll(hid[:, width:], -1, axis=0)
    gate_sig = jax.nn.sigmoid(gate_pre)
    first = lax.broadcasted_iota(jnp.int32, (2 * slots, 1), 0) % 2 == 0

    def kept(values):
        return jnp.where(first, values, 0.0).astype(jnp.bfloat16)

    hidden = kept(gate_pre * gate_sig * up_pre)
    grad_up_act = kept(grad_hidden * gate_pre * gate_sig)
    grad_gate_act = kept(grad_hidden * up_pre * gate_sig * (1.0 + gate_pre * (1.0 - gate_sig)))
    acts = jnp.concatenate([grad_gate_act, grad_up_act], axis=1)
    pick = (
        lax.broadcasted_iota(jnp.int32, (slots, 2 * slots), 1)
        == 2 * lax.broadcasted_iota(jnp.int32, (slots, 2 * slots), 0)
    ).astype(jnp.bfloat16)
    acts = jnp.dot(pick, acts, preferred_element_type=jnp.float32).astype(jnp.bfloat16)
    out_w = jnp.concatenate([gate_w, up_w], axis=1).reshape(y_count, 2, width, 2 * width)
    out_own = jnp.where(core == 0, out_w[:, 0], out_w[:, 1]).reshape(half, 2 * width)
    out_other = jnp.where(core == 0, out_w[:, 1], out_w[:, 0]).reshape(half, 2 * width)

    def onto(weights):
        return lax.dot_general(
            acts, weights, (((1,), (1,)), ((), ())), preferred_element_type=jnp.float32
        )

    passed = lax.ppermute(onto(out_other).astype(jnp.bfloat16), "c", [(0, 1), (1, 0)])
    pair_sum = (onto(out_own) + passed.astype(jnp.float32)).astype(jnp.bfloat16)
    parts = pair_sum.reshape(slots, y_count, width).transpose(1, 0, 2)
    summed = sum_parts(lax.all_to_all(parts, "y", 0, 0, tiled=True)).astype(jnp.bfloat16)

    def beside(values):
        return jnp.concatenate([values, jnp.roll(values, 1, axis=0)], axis=1)

    grad_in_w = lax.dot_general(
        rows_in,
        jnp.concatenate([beside(grad_gate_act), beside(grad_up_act)], axis=1),
        (((0,), (0,)), ((), ())),
        preferred_element_type=jnp.float32,
    ).astype(jnp.bfloat16)
    grad_gate_w = jnp.concatenate([grad_in_w[:, :width], grad_in_w[:, width : 2 * width]], axis=0)
    grad_up_w = jnp.concatenate(
        [grad_in_w[:, 2 * width : 3 * width], grad_in_w[:, 3 * width :]], axis=0
    )
    grad_out_w = lax.dot_general(
        beside(hidden), rows_cot, (((0,), (0,)), ((), ())), preferred_element_type=jnp.float32
    ).astype(jnp.bfloat16)
    grad_down_w = jnp.concatenate([grad_out_w[:width], grad_out_w[width:]], axis=1)
    out_proj_here, own_tied = lax.optimization_barrier((out_proj, rows_in))
    out_proj_all = to_all(out_proj_here, SP).reshape(model_width, -1)
    returned = lax.all_to_all(
        summed.reshape(experts, capacity, -1), SP, split_axis=0, concat_axis=0, tiled=True
    )
    flat_rows = returned.reshape(slots, -1)
    slot_index = lax.broadcasted_iota(jnp.int32, (slots, tokens_here), 0)
    slot_tokens = ((slot_index == slot_a[None, :]) | (slot_index == slot_b[None, :])).astype(
        jnp.bfloat16
    )
    grad_normed = lax.all_gather(
        lax.dot_general(
            slot_tokens, flat_rows, (((0,), (0,)), ((), ())), preferred_element_type=jnp.float32
        ).astype(jnp.bfloat16),
        ("y", "c"),
        axis=1,
        tiled=True,
    ).astype(jnp.float32)
    scaled = grad_normed * norm_gain
    grad_resid = cotangent.astype(jnp.float32) + inverse_rms * (
        scaled - unit_rows * jnp.mean(scaled * unit_rows, axis=1, keepdims=True)
    )
    grad_resid = grad_resid.astype(jnp.bfloat16)
    grad_mixed = jnp.dot(grad_resid, out_proj_all, preferred_element_type=jnp.float32).astype(
        jnp.bfloat16
    )
    share = lax.dot_general(
        grad_resid, mixed, (((0,), (0,)), ((), ())), preferred_element_type=jnp.float32
    ).astype(jnp.bfloat16)
    grad_out_proj = sum_parts(
        lax.all_to_all(share.reshape(sp_count, model_width // sp_count, -1), SP, 0, 0, tiled=True)
    )
    head_count = query.shape[1] // KEY_CHANNELS
    query_scale = KEY_CHANNELS ** (-0.5)

    def heads_first(values, head_depth):
        return values.reshape(tokens_here, head_count, head_depth).transpose(1, 0, 2)

    query_rows = heads_first(query, KEY_CHANNELS).astype(jnp.float32) * query_scale
    key_rows = heads_first(key, KEY_CHANNELS).astype(jnp.float32)
    value_rows = heads_first(value, DV).astype(jnp.float32)
    grad_rows = heads_first(grad_mixed, DV).astype(jnp.float32)
    decay_rows = heads_first(log_decay, KEY_CHANNELS)
    kept_terms, summary = jax.vmap(span_forward)(
        query_rows, key_rows, value_rows, grad_rows, decay_rows, span_state[0]
    )
    own_decay, own_state = (summary[0][0], summary[1][0])
    near_states, near_decays = split_decay(to_all(with_decay(own_state, own_decay), "x"))
    near_sum, near_factor = later_sum(near_states, near_decays, lax.axis_index("x"))
    group_sum, group_factor = later_sum(near_states, near_decays, -1)
    far_states, far_decays = split_decay(to_all(with_decay(group_sum, group_factor), "z"))
    far_sum, _ = later_sum(far_states, far_decays, lax.axis_index("z"))
    exit_cot = near_sum + near_factor[:, None] * far_sum
    head_grads = jax.vmap(span_backward)(
        query_rows, key_rows, value_rows, grad_rows, kept_terms, exit_cot[None]
    )

    def tokens_first(values):
        return values.transpose(1, 0, 2).reshape(tokens_here, -1)

    grad_query = (tokens_first(head_grads[0]) * query_scale).astype(jnp.bfloat16)
    grad_key = tokens_first(head_grads[1]).astype(jnp.bfloat16)
    grad_value = tokens_first(head_grads[2]).astype(jnp.bfloat16)
    grad_log_decay = tokens_first(head_grads[3])
    return (
        grad_gate_w[None],
        grad_up_w[None],
        grad_down_w[None],
        grad_out_proj,
        grad_query,
        grad_key,
        grad_value,
        grad_log_decay,
    )


def solution(mesh):
    finer = Mesh(mesh.devices.reshape(8, 4, 8, 2), ("z", "x", "y", "c"))
    in_specs = (
        P(SP, None),
        P(),
        P(SP, None),
        P(SP, None),
        P(SP, None),
        P(SP, None, TP),
        P(SP, None, TP),
        P(SP, TP, None),
        P(SP, TP),
        P(SP, TP),
        P(SP, TP),
        P(SP, TP),
        P(SP, TP),
        P(SP, TP),
        P(SP, TP, None, None),
    )
    out_specs = (
        P(SP, None, TP),
        P(SP, None, TP),
        P(SP, TP, None),
        P(SP, TP),
        P(SP, TP),
        P(SP, TP),
        P(SP, TP),
        P(SP, TP),
    )
    return jax.shard_map(
        on_device, mesh=finer, in_specs=in_specs, out_specs=out_specs, check_vma=False
    )
```

profile of v0, /device:TPU:2, one launch (start us, length us, event | category | flops | bytes accessed | tf_op | source)
XLA Modules:
  0.0 222.4 jit_solution(10590077181551964781)
XLA Ops:
  0.7 0.9 copy.91
  1.8 0.8 slice_bitcast_fusion.11
  3.7 0.7 multiply_add_fusion
  4.5 1.2 fusion.22
  6.2 1.0 fusion.48
  7.2 1.8 multiply_convert_fusion
  9.0 13.6 %all-to-all-start = ((bf16[32,24,1024]{2,1,0:T(8,128)(2,1)}), bf16[32,24,1024]{2,1,0:T(8,128)(2,1)S(1)}, u32[]{:S(2)}, u32[]{:S(2)}) async-start(bf16[32,24,1024]{2,1,0:T(8,128)(2,1)} %bitcast.383), calls=%async_computation | async-start | bytes 3145728 | tf_op jit(solution)/shard_map/all_to_all | solution.py:168
  25.3 35.7 %all-to-all-done = bf16[32,24,1024]{2,1,0:T(8,128)(2,1)S(1)} async-done(((bf16[32,24,1024]{2,1,0:T(8,128)(2,1)}), bf16[32,24,1024]{2,1,0:T(8,128)(2,1)S(1)}, u32[]{:S(2)}, u32[]{:S(2)}) %all-to-all-start) | async-done | bytes 1572896 | tf_op jit(solution)/shard_map/all_to_all | solution.py:168
  61.0 1.9 collective-permute-start
  63.0 2.3 %broadcast_select_fusion.4 = (bf16[8,1,128,256]{3,2,1,0:T(8,128)(2,1)S(1)}, bf16[8,1,128,256]{3,2,1,0:T(8,128)(2,1)}) fusion(pred[]{:T(512)S(6)} %eq.83, bf16[8,2,128,128]{3,2,1,0:T(8,128)(2,1)S(1)} %bitcast.376, bf16[8,2,128,128]{3,2,1,0:T(8,128)(2,1)} %bitcast.377), kind=kLoop, calls=%fused_computation.94 | loop fusion | flops 3670016 | bytes 2097153 | tf_op jit(solution)/shard_map/jit(_where)/select_n | solution.py:200
  67.0 1.0 fusion.23
  68.2 2.0 fusion.45
  70.3 0.9 select_convert_fusion
  72.2 1.3 convolution_convert_fusion.2
  73.5 2.3 %collective-permute-start.1 = (bf16[384,1024]{1,0:T(8,128)(2,1)}, bf16[384,1024]{1,0:T(8,128)(2,1)}, u32[]{:S(2)}, u32[]{:S(2)}) collective-permute-start(bf16[384,1024]{1,0:T(8,128)(2,1)} %convolution_convert_fusion.2), channel_id=1, source_target_pairs={{0,1},{1,0},{2,3},{3,2},{4,5},{5,4},{6,7},{7,6},{8,9},{9,8},{10,11... | collective-permute-start | bytes 2359304 | tf_op jit(solution)/shard_map/ppermute | solution.py:207
  75.8 1.5 while.29
  78.0 1.5 fusion.31
  79.6 1.1 copy.125
  80.7 7.1 %all-to-all-start.1 = ((bf16[8,384,128]{2,1,0:T(8,128)(2,1)}), bf16[8,384,128]{2,1,0:T(8,128)(2,1)S(1)}, u32[]{:S(2)}, u32[]{:S(2)}) async-start(bf16[8,384,128]{2,1,0:T(8,128)(2,1)} %bitcast.374), calls=%async_computation.1 | async-start | bytes 1572864 | tf_op jit(solution)/shard_map/all_to_all | solution.py:210
  87.9 4.4 %fusion.4 = (bf16[2,64,64]{2,1,0:T(8,128)(2,1)}, f32[2,64,128,64]{2,3,1,0:T(8,128)}) fusion(f32[2,128,64]{1,2,0:T(8,128)S(1)} %copy-done.21, f32[2,128,64]{1,2,0:T(8,128)S(1)} %bitcast.384, f32[2,64,128]{2,1,0:T(8,128)S(1)} %bitcast.371, pred[64,64]{1,0:T(8,128)(4,1)S(1)} %iota_compare_fusion.10), kind=kLoop, calls=%fused_computation.11 | loop fusion | flops 5234688 | bytes 4411392 | tf_op jit(solution)/shard_map/vmap(ntd,nsd,ntsd->nts)/dot_general | solution.py:91
  92.3 1.0 convolution_convert_fusion.1
  93.3 1.0 fusion.147
  94.3 2.8 %convolution_convert_fusion.3 = bf16[256,1024]{1,0:T(8,128)(2,1)} fusion(bf16[768,1024]{1,0:T(8,128)(2,1)} %collective-permute-done, bf16[768,1024]{1,0:T(8,128)(2,1)S(1)} %bitcast.370, pred[]{:T(512)S(6)} %eq.83, bf16[767,128]{1,0:T(8,128)(2,1)S(1)} %bitcast.395, bf16[1,128]{1,0:T(2,128)(2,1)S(1)} %slice.339, bf16[768,128]{1,0:T(8,128)(2,1)S(1)} %copy-done.22), kind=kOutput, calls=%fused_computation.30 | convolution fusion | flops 404881408 | bytes 4063233 | tf_op jit(solution)/shard_map/dot_general | solution.py:225
  97.1 14.4 %all-to-all-done.1 = bf16[8,384,128]{2,1,0:T(8,128)(2,1)S(1)} async-done(((bf16[8,384,128]{2,1,0:T(8,128)(2,1)}), bf16[8,384,128]{2,1,0:T(8,128)(2,1)S(1)}, u32[]{:S(2)}, u32[]{:S(2)}) %all-to-all-start.1) | async-done | bytes 786464 | tf_op jit(solution)/shard_map/all_to_all | solution.py:210
  111.6 0.7 reshape.961
  112.3 6.5 %all-to-all-start.2 = ((bf16[32,12,128]{2,1,0:T(8,128)(2,1)}), bf16[32,12,128]{2,1,0:T(8,128)(2,1)S(1)}, u32[]{:S(2)}, u32[]{:S(2)}) async-start(bf16[32,12,128]{2,1,0:T(8,128)(2,1)} %reshape.961), calls=%async_computation.2 | async-start | bytes 262144 | tf_op jit(solution)/shard_map/all_to_all | solution.py:231
  118.8 1.9 maximum_bitcast_fusion
  120.7 7.1 %all-to-all-done.2 = bf16[32,12,128]{2,1,0:T(8,128)(2,1)S(1)} async-done(((bf16[32,12,128]{2,1,0:T(8,128)(2,1)}), bf16[32,12,128]{2,1,0:T(8,128)(2,1)S(1)}, u32[]{:S(2)}, u32[]{:S(2)}) %all-to-all-start.2) | async-done | bytes 98336 | tf_op jit(solution)/shard_map/all_to_all | solution.py:231
  127.8 1.2 broadcast_in_dim.169
  129.0 5.6 %all-to-all-start.4 = ((bf16[32,64,256]{2,1,0:T(8,128)(2,1)}), bf16[32,64,256]{2,1,0:T(8,128)(2,1)S(1)}, u32[]{:S(2)}, u32[]{:S(2)}) async-start(bf16[32,64,256]{2,1,0:T(8,128)(2,1)} %broadcast_in_dim.169), calls=%async_computation.4 | async-start | bytes 2097152 | tf_op jit(solution)/shard_map/all_to_all | solution.py:34
  134.6 0.8 maximum_bitcast_fusion.1
  135.5 0.8 maximum_bitcast_fusion.2
  136.7 16.1 %all_gather.3 = bf16[128,2048]{1,0:T(8,128)(2,1)S(1)} all-gather(bf16[128,128]{1,0:T(8,128)(2,1)S(1)} %convolution_convert_fusion.5), channel_id=1, replica_groups=mesh['z'=8,'x'=4,'y'=8,'c'=2] {'y','c'}, dimensions={1}, use_global_device_ids=true | all-gather | bytes 557056 | tf_op jit(solution)/shard_map/all_gather | solution.py:239
  153.6 8.0 %all-to-all-done.4 = bf16[32,64,256]{2,1,0:T(8,128)(2,1)S(1)} async-done(((bf16[32,64,256]{2,1,0:T(8,128)(2,1)}), bf16[32,64,256]{2,1,0:T(8,128)(2,1)S(1)}, u32[]{:S(2)}, u32[]{:S(2)}) %all-to-all-start.4) | async-done | bytes 1048608 | tf_op jit(solution)/shard_map/all_to_all | solution.py:34
  162.8 0.7 broadcast_in_dim.173
  163.5 4.9 %all-to-all-start.5 = ((bf16[4,136,256]{2,1,0:T(8,128)(2,1)}), bf16[4,136,256]{2,1,0:T(8,128)(2,1)S(1)}, u32[]{:S(2)}, u32[]{:S(2)}) async-start(bf16[4,136,256]{2,1,0:T(8,128)(2,1)} %broadcast_in_dim.173), calls=%async_computation.5 | async-start | bytes 557056 | tf_op jit(solution)/shard_map/all_to_all | solution.py:34
  168.7 5.1 %all-to-all-done.5 = bf16[4,136,256]{2,1,0:T(8,128)(2,1)S(1)} async-done(((bf16[4,136,256]{2,1,0:T(8,128)(2,1)}), bf16[4,136,256]{2,1,0:T(8,128)(2,1)S(1)}, u32[]{:S(2)}, u32[]{:S(2)}) %all-to-all-start.5) | async-done | bytes 278560 | tf_op jit(solution)/shard_map/all_to_all | solution.py:34
  174.0 0.9 broadcast_in_dim.175
  174.8 3.5 %all-to-all-start.6 = ((bf16[8,136,256]{2,1,0:T(8,128)(2,1)}), bf16[8,136,256]{2,1,0:T(8,128)(2,1)S(1)}, u32[]{:S(2)}, u32[]{:S(2)}) async-start(bf16[8,136,256]{2,1,0:T(8,128)(2,1)} %broadcast_in_dim.175), calls=%async_computation.6 | async-start | bytes 1114112 | tf_op jit(solution)/shard_map/all_to_all | solution.py:34
  178.4 5.0 %fusion.5 = f32[2,64,128]{2,1,0:T(8,128)S(1)} fusion(f32[2,64,128,64]{2,3,1,0:T(8,128)} %get-tuple-element.289, f32[2,64,128]{2,1,0:T(8,128)S(1)} %copy-done.20, f32[2,64,64]{2,1,0:T(8,128)S(1)} %copy.98), kind=kLoop, calls=%fused_computation.13 | loop fusion | flops 3129344 | bytes 4358144 | tf_op jit(solution)/shard_map/vmap(nts,nsd,ntsd->ntd)/dot_general | solution.py:94
  183.6 1.4 convolution_convert_fusion
  185.0 2.0 multiply_reduce_fusion
  187.0 6.0 %all-to-all-done.6 = bf16[8,136,256]{2,1,0:T(8,128)(2,1)S(1)} async-done(((bf16[8,136,256]{2,1,0:T(8,128)(2,1)}), bf16[8,136,256]{2,1,0:T(8,128)(2,1)S(1)}, u32[]{:S(2)}, u32[]{:S(2)}) %all-to-all-start.6) | async-done | bytes 557088 | tf_op jit(solution)/shard_map/all_to_all | solution.py:34
  193.0 5.0 %all-to-all-start.3 = ((bf16[32,64,256]{2,1,0:T(8,128)(2,1)}), bf16[32,64,256]{2,1,0:T(8,128)(2,1)S(1)}, u32[]{:S(2)}, u32[]{:S(2)}) async-start(bf16[32,64,256]{2,1,0:T(8,128)(2,1)} %bitcast.28), calls=%async_computation.3 | async-start | bytes 2097152 | tf_op jit(solution)/shard_map/all_to_all | solution.py:259
  198.4 0.9 multiply_subtract_fusion
  200.7 0.8 fusion.12
  201.6 20.1 %all-to-all-done.3 = bf16[32,64,256]{2,1,0:T(8,128)(2,1)S(1)} async-done(((bf16[32,64,256]{2,1,0:T(8,128)(2,1)}), bf16[32,64,256]{2,1,0:T(8,128)(2,1)S(1)}, u32[]{:S(2)}, u32[]{:S(2)}) %all-to-all-start.3) | async-done | bytes 1048608 | tf_op jit(solution)/shard_map/all_to_all | solution.py:259
  221.6 0.8 convert_reduce_fusion
  (173 shorter events, 14.7 us)
Async XLA Ops:
  0.6 182.9 %copy-start = (bf16[128,256]{1,0:T(8,128)(2,1)S(1)}, bf16[128,256]{1,0:T(8,128)(2,1)}, u32[]{:S(2)}) copy-start(bf16[128,256]{1,0:T(8,128)(2,1)} %param.28) | copy-start | bytes 196612
  0.6 5.5 %copy-start.2 = (bf16[128,2048]{1,0:T(8,128)(2,1)S(1)}, bf16[128,2048]{1,0:T(8,128)(2,1)}, u32[]{:S(2)}) copy-start(bf16[128,2048]{1,0:T(8,128)(2,1)} %param.19) | copy-start | bytes 1572868
  0.7 5.5 %copy-start.6 = (bf16[128,2048]{1,0:T(8,128)(2,1)S(1)}, bf16[128,2048]{1,0:T(8,128)(2,1)}, u32[]{:S(2)}) copy-start(bf16[128,2048]{1,0:T(8,128)(2,1)} %param.21) | copy-start | bytes 1572868
  9.0 13.6 %copy-start.31 = (f32[128,128]{1,0:T(8,128)S(1)}, f32[128,128]{1,0:T(8,128)}, u32[]{:S(2)}) copy-start(f32[128,128]{1,0:T(8,128)} %param.32) | copy-start | bytes 196612
  9.0 15.6 %copy-start.13 = (bf16[128,256]{1,0:T(8,128)(2,1)S(1)}, bf16[128,256]{1,0:T(8,128)(2,1)}, u32[]{:S(2)}) copy-start(bf16[128,256]{1,0:T(8,128)(2,1)} %param.31) | copy-start | bytes 196612
  9.0 15.6 %copy-start.18 = (bf16[128,128]{1,0:T(8,128)(2,1)S(1)}, bf16[128,128]{1,0:T(8,128)(2,1)}, u32[]{:S(2)}) copy-start(bf16[128,128]{1,0:T(8,128)(2,1)} %param.30) | copy-start | bytes 98308
  9.0 54.0 %copy-start.3 = (bf16[1,2048,128]{2,1,0:T(8,128)(2,1)S(1)}, bf16[1,2048,128]{2,1,0:T(8,128)(2,1)}, u32[]{:S(2)}) copy-start(bf16[1,2048,128]{2,1,0:T(8,128)(2,1)} %param.25) | copy-start | bytes 1572868
  9.0 52.0 %all-to-all-start = ((bf16[32,24,1024]{2,1,0:T(8,128)(2,1)}), bf16[32,24,1024]{2,1,0:T(8,128)(2,1)S(1)}, u32[]{:S(2)}, u32[]{:S(2)}) async-start(bf16[32,24,1024]{2,1,0:T(8,128)(2,1)} %bitcast.383), calls=%async_computation | async-start | bytes 3145728 | tf_op jit(solution)/shard_map/all_to_all | solution.py:168
  22.6 43.2 %copy-start.28 = (bf16[128,128]{1,0:T(8,128)(2,1)S(1)}, bf16[128,128]{1,0:T(8,128)(2,1)}, u32[]{:S(2)}) copy-start(bf16[128,128]{1,0:T(8,128)(2,1)} %param.29) | copy-start | bytes 98308
  61.0 5.7 %collective-permute-start = (bf16[768,1024]{1,0:T(8,128)(2,1)S(1)}, bf16[768,1024]{1,0:T(8,128)(2,1)}, u32[]{:S(2)}, u32[]{:S(2)}) collective-permute-start(bf16[768,1024]{1,0:T(8,128)(2,1)S(1)} %bitcast.368), channel_id=1, source_target_pairs={{0,1},{1,0},{2,3},{3,2},{4,5},{5,4},{6,7},{7,6},{8,9},{9,8},{10,11... | collective-permute-start | bytes 4718600 | tf_op jit(solution)/shard_map/ppermute | solution.py:169
  62.9 3.6 %copy-start.16 = (bf16[1,128,2048]{2,1,0:T(8,128)(2,1)S(1)}, bf16[1,128,2048]{2,1,0:T(8,128)(2,1)}, u32[]{:S(2)}) copy-start(bf16[1,128,2048]{2,1,0:T(8,128)(2,1)} %param.26) | copy-start | bytes 1572868
  63.0 3.6 %copy-start.4 = (bf16[1,2048,128]{2,1,0:T(8,128)(2,1)S(1)}, bf16[1,2048,128]{2,1,0:T(8,128)(2,1)}, u32[]{:S(2)}) copy-start(bf16[1,2048,128]{2,1,0:T(8,128)(2,1)} %param.24) | copy-start | bytes 1572868
  65.9 21.9 %copy-start.11 = (f32[128,128]{1,0:T(8,128)}, f32[128,128]{1,0:T(8,128)S(1)}, u32[]{:S(2)}) copy-start(f32[128,128]{1,0:T(8,128)S(1)} %convert_multiply_fusion.18) | copy-start | bytes 196612
  67.0 1.1 copy-start.8
  71.1 0.7 copy-start.35
  71.4 4.4 %copy-start.23 = (bf16[768,128]{1,0:T(8,128)(2,1)}, bf16[768,128]{1,0:T(8,128)(2,1)S(1)}, u32[]{:S(2)}) copy-start(bf16[768,128]{1,0:T(8,128)(2,1)S(1)} %get-tuple-element.266) | copy-start | bytes 589828
  71.4 4.4 %copy-start.25 = (bf16[768,128]{1,0:T(8,128)(2,1)}, bf16[768,128]{1,0:T(8,128)(2,1)S(1)}, u32[]{:S(2)}) copy-start(bf16[768,128]{1,0:T(8,128)(2,1)S(1)} %get-tuple-element.267) | copy-start | bytes 589828
  71.4 4.4 %copy-start.1 = (f32[1,1,128,256]{3,2,1,0:T(8,128)S(1)}, f32[1,1,128,256]{3,2,1,0:T(8,128)}, u32[]{:S(2)}) copy-start(f32[1,1,128,256]{3,2,1,0:T(8,128)} %param.33) | copy-start | bytes 393220
  71.5 4.4 %copy-start.36 = (f32[2,1,128]{2,1,0:T(1,128)S(1)}, f32[2,1,128]{2,1,0:T(1,128)}, u32[]{:S(2)}) copy-start(f32[2,1,128]{2,1,0:T(1,128)} %get-tuple-element.408) | copy-start | bytes 3076
  73.5 4.5 %collective-permute-start.1 = (bf16[384,1024]{1,0:T(8,128)(2,1)}, bf16[384,1024]{1,0:T(8,128)(2,1)}, u32[]{:S(2)}, u32[]{:S(2)}) collective-permute-start(bf16[384,1024]{1,0:T(8,128)(2,1)} %convolution_convert_fusion.2), channel_id=1, source_target_pairs={{0,1},{1,0},{2,3},{3,2},{4,5},{5,4},{6,7},{7,6},{8,9},{9,8},{10,11... | collective-permute-start | bytes 2359304 | tf_op jit(solution)/shard_map/ppermute | solution.py:207
  75.8 2.2 copy-start.5
  79.6 8.2 %copy-start.21 = (f32[2,128,64]{1,2,0:T(8,128)S(1)}, f32[2,128,64]{1,2,0:T(8,128)}, u32[]{:S(2)}) copy-start(f32[2,128,64]{1,2,0:T(8,128)} %get-tuple-element.296) | copy-start | bytes 196612
  80.7 30.8 %all-to-all-start.1 = ((bf16[8,384,128]{2,1,0:T(8,128)(2,1)}), bf16[8,384,128]{2,1,0:T(8,128)(2,1)S(1)}, u32[]{:S(2)}, u32[]{:S(2)}) async-start(bf16[8,384,128]{2,1,0:T(8,128)(2,1)} %bitcast.374), calls=%async_computation.1 | async-start | bytes 1572864 | tf_op jit(solution)/shard_map/all_to_all | solution.py:210
  87.8 4.4 %copy-start.26 = (bf16[768,128]{1,0:T(8,128)(2,1)S(1)}, bf16[768,128]{1,0:T(8,128)(2,1)}, u32[]{:S(2)}) copy-start(bf16[768,128]{1,0:T(8,128)(2,1)} %copy-done.25) | copy-start | bytes 589828
  87.8 4.4 %copy-start.24 = (bf16[768,128]{1,0:T(8,128)(2,1)S(1)}, bf16[768,128]{1,0:T(8,128)(2,1)}, u32[]{:S(2)}) copy-start(bf16[768,128]{1,0:T(8,128)(2,1)} %copy-done.23) | copy-start | bytes 589828
  87.8 4.4 %copy-start.22 = (bf16[768,128]{1,0:T(8,128)(2,1)S(1)}, bf16[768,128]{1,0:T(8,128)(2,1)}, u32[]{:S(2)}) copy-start(bf16[768,128]{1,0:T(8,128)(2,1)} %get-tuple-element.264) | copy-start | bytes 589828
  87.8 4.4 %copy-start.9 = (bf16[768,1024]{1,0:T(8,128)(2,1)S(1)}, bf16[768,1024]{1,0:T(8,128)(2,1)}, u32[]{:S(2)}) copy-start(bf16[768,1024]{1,0:T(8,128)(2,1)} %copy-done.8) | copy-start | bytes 4718596
  97.1 30.7 %copy-start.32 = (bf16[64,256]{1,0:T(8,128)(2,1)S(1)}, bf16[64,256]{1,0:T(8,128)(2,1)}, u32[]{:S(2)}) copy-start(bf16[64,256]{1,0:T(8,128)(2,1)} %param.27) | copy-start | bytes 98308
  112.3 15.5 %all-to-all-start.2 = ((bf16[32,12,128]{2,1,0:T(8,128)(2,1)}), bf16[32,12,128]{2,1,0:T(8,128)(2,1)S(1)}, u32[]{:S(2)}, u32[]{:S(2)}) async-start(bf16[32,12,128]{2,1,0:T(8,128)(2,1)} %reshape.961), calls=%async_computation.2 | async-start | bytes 262144 | tf_op jit(solution)/shard_map/all_to_all | solution.py:231
  120.7 13.9 %copy-start.10 = (bf16[1024,128]{1,0:T(8,128)(2,1)S(1)}, bf16[1024,128]{1,0:T(8,128)(2,1)}, u32[]{:S(2)}) copy-start(bf16[1024,128]{1,0:T(8,128)(2,1)} %get-tuple-element.275) | copy-start | bytes 786436
  129.0 6.5 %copy-start.17 = (bf16[256,1024]{1,0:T(8,128)(2,1)S(1)}, bf16[256,1024]{1,0:T(8,128)(2,1)}, u32[]{:S(2)}) copy-start(bf16[256,1024]{1,0:T(8,128)(2,1)} %convolution_convert_fusion.3) | copy-start | bytes 1572868
  129.0 32.6 %all-to-all-start.4 = ((bf16[32,64,256]{2,1,0:T(8,128)(2,1)}), bf16[32,64,256]{2,1,0:T(8,128)(2,1)S(1)}, u32[]{:S(2)}, u32[]{:S(2)}) async-start(bf16[32,64,256]{2,1,0:T(8,128)(2,1)} %broadcast_in_dim.169), calls=%async_computation.4 | async-start | bytes 2097152 | tf_op jit(solution)/shard_map/all_to_all | solution.py:34
  134.6 1.8 copy-start.39
  134.6 1.8 copy-start.40
  135.5 17.3 %copy-start.30 = (f32[2048]{0:T(1024)S(1)}, f32[2048]{0:T(1024)}, u32[]{:S(2)}) copy-start(f32[2048]{0:T(1024)} %param.20) | copy-start | bytes 24580
  135.5 17.3 %copy-start.34 = (f32[128]{0:T(128)S(1)}, f32[128]{0:T(128)}, u32[]{:S(2)}) copy-start(f32[128]{0:T(128)} %copy-done.33) | copy-start | bytes 1540
  135.5 17.6 %copy-start.7 = (bf16[128,2048]{1,0:T(8,128)(2,1)S(1)}, bf16[128,2048]{1,0:T(8,128)(2,1)}, u32[]{:S(2)}) copy-start(bf16[128,2048]{1,0:T(8,128)(2,1)} %param.21) | copy-start | bytes 1572868
  153.1 8.8 %copy-start.12 = (f32[128,128]{1,0:T(8,128)S(1)}, f32[128,128]{1,0:T(8,128)}, u32[]{:S(2)}) copy-start(f32[128,128]{1,0:T(8,128)} %copy-done.11) | copy-start | bytes 196612
  153.6 8.6 %copy-start.37 = (f32[2,1,128]{2,1,0:T(1,128)S(1)}, f32[2,1,128]{2,1,0:T(1,128)}, u32[]{:S(2)}) copy-start(f32[2,1,128]{2,1,0:T(1,128)} %get-tuple-element.408) | copy-start | bytes 3076
  162.2 6.3 %copy-start.14 = (bf16[128,256]{1,0:T(8,128)(2,1)S(1)}, bf16[128,256]{1,0:T(8,128)(2,1)}, u32[]{:S(2)}) copy-start(bf16[128,256]{1,0:T(8,128)(2,1)} %param.31) | copy-start | bytes 196612
  163.5 14.8 %copy-start.20 = (f32[2,64,128]{2,1,0:T(8,128)S(1)}, f32[2,64,128]{2,1,0:T(8,128)}, u32[]{:S(2)}) copy-start(f32[2,64,128]{2,1,0:T(8,128)} %get-tuple-element.297) | copy-start | bytes 196612
  163.5 10.2 %all-to-all-start.5 = ((bf16[4,136,256]{2,1,0:T(8,128)(2,1)}), bf16[4,136,256]{2,1,0:T(8,128)(2,1)S(1)}, u32[]{:S(2)}, u32[]{:S(2)}) async-start(bf16[4,136,256]{2,1,0:T(8,128)(2,1)} %broadcast_in_dim.173), calls=%async_computation.5 | async-start | bytes 557056 | tf_op jit(solution)/shard_map/all_to_all | solution.py:34
  174.8 18.2 %all-to-all-start.6 = ((bf16[8,136,256]{2,1,0:T(8,128)(2,1)}), bf16[8,136,256]{2,1,0:T(8,128)(2,1)S(1)}, u32[]{:S(2)}, u32[]{:S(2)}) async-start(bf16[8,136,256]{2,1,0:T(8,128)(2,1)} %broadcast_in_dim.175), calls=%async_computation.6 | async-start | bytes 1114112 | tf_op jit(solution)/shard_map/all_to_all | solution.py:34
  178.4 5.0 %copy-start.15 = (bf16[2,1,128,256]{3,2,1,0:T(8,128)(2,1)S(1)}, bf16[2,1,128,256]{3,2,1,0:T(8,128)(2,1)}, u32[]{:S(2)}) copy-start(bf16[2,1,128,256]{3,2,1,0:T(8,128)(2,1)} %get-tuple-element.142) | copy-start | bytes 393220
  187.0 11.4 %copy-start.19 = (bf16[128,128]{1,0:T(8,128)(2,1)S(1)}, bf16[128,128]{1,0:T(8,128)(2,1)}, u32[]{:S(2)}) copy-start(bf16[128,128]{1,0:T(8,128)(2,1)} %param.30) | copy-start | bytes 98308
  187.0 11.4 %copy-start.29 = (bf16[128,128]{1,0:T(8,128)(2,1)S(1)}, bf16[128,128]{1,0:T(8,128)(2,1)}, u32[]{:S(2)}) copy-start(bf16[128,128]{1,0:T(8,128)(2,1)} %param.29) | copy-start | bytes 98308
  193.0 28.6 %all-to-all-start.3 = ((bf16[32,64,256]{2,1,0:T(8,128)(2,1)}), bf16[32,64,256]{2,1,0:T(8,128)(2,1)S(1)}, u32[]{:S(2)}, u32[]{:S(2)}) async-start(bf16[32,64,256]{2,1,0:T(8,128)(2,1)} %bitcast.28), calls=%async_computation.3 | async-start | bytes 2097152 | tf_op jit(solution)/shard_map/all_to_all | solution.py:259
  198.4 2.3 %copy-start.27 = (bf16[2,64,64]{2,1,0:T(8,128)(2,1)S(1)}, bf16[2,64,64]{2,1,0:T(8,128)(2,1)}, u32[]{:S(2)}) copy-start(bf16[2,64,64]{2,1,0:T(8,128)(2,1)} %get-tuple-element.288) | copy-start | bytes 49156
  (2 other events, 1.1 us)
where the time goes:
time: 224 us; the launch traced here: 222 us
  waiting for transfers between devices  97 us (43%)
  starting transfers between devices  50.6 us (23%)
  other arithmetic  29.2 us (13%)
  matrix products  16.6 us (7%)
  blocking collectives  16.1 us (7%)
  local copies, waits for them, and re-layouts  11.3 us (5%)
    all_to_all x1, waiting for transfers between devices, on_device(): own = lax.all_to_all(sent, SP, 0, 0, tiled=True).reshape(2 * slots, half)  35.7 us
    all_to_all x1, waiting for transfers between devices, on_device(): lax.all_to_all(share.reshape(sp_count, model_width // sp_count, -1), SP,...  20.1 us
    all_to_all x3, waiting for transfers between devices, to_all(): return lax.all_to_all(copies, axis, 0, 0, tiled=True)  19.1 us
    all_gather x1, blocking collectives, on_device(): lax.all_gather(lax.dot_general(slot_tokens, flat_rows, (((0,), (0,)), (()...  16.1 us
    all_to_all x1, waiting for transfers between devices, on_device(): lax.all_to_all(parts, 'y', 0, 0, tiled=True)  14.4 us
    all_to_all x3, starting transfers between devices, to_all(): return lax.all_to_all(copies, axis, 0, 0, tiled=True)  14.1 us
    all_to_all x1, starting transfers between devices, on_device(): own = lax.all_to_all(sent, SP, 0, 0, tiled=True).reshape(2 * slots, half)  13.6 us
    all_to_all x1, waiting for transfers between devices, on_device(): lax.all_to_all(summed.reshape(experts, capacity, -1), SP, split_axis=0, c...  7.14 us
  transfers between devices with their start and end apart: 9, of which 8 were waited for; matrix products, arithmetic and copies ran while one was open for 15% of the time, Pallas kernels for 0%

commit v1 on v0

--- a/solution.py
+++ b/solution.py
@@ -236,13 +236,24 @@
     slot_tokens = ((slot_index == slot_a[None, :]) | (slot_index == slot_b[None, :])).astype(
         jnp.bfloat16
     )
-    grad_normed = lax.all_gather(
-        lax.dot_general(
-            slot_tokens, flat_rows, (((0,), (0,)), ((), ())), preferred_element_type=jnp.float32
-        ).astype(jnp.bfloat16),
-        ("y", "c"),
+    grad_normed = jnp.concatenate(
+        lax.all_to_all(
+            jnp.stack(
+                [
+                    lax.dot_general(
+                        slot_tokens,
+                        flat_rows,
+                        (((0,), (0,)), ((), ())),
+                        preferred_element_type=jnp.float32,
+                    ).astype(jnp.bfloat16)
+                ]
+                * lax.axis_size(("y", "c"))
+            ),
+            ("y", "c"),
+            0,
+            0,
+        ),
         axis=1,
-        tiled=True,
     ).astype(jnp.float32)
     scaled = grad_normed * norm_gain
     grad_resid = cotangent.astype(jnp.float32) + inverse_rms * (

time: 224 us -> 254 us (1.13)
  blocking collectives: 16.1 us -> 52.7 us
  starting transfers between devices: 50.6 us -> 40.7 us
  local copies, waits for them, and re-layouts: 11.3 us -> 14.2 us
  matrix products: 16.6 us -> 13.8 us
    all_to_all x0 -> x1, blocking collectives: none -> 52.7 us  [on_device(): own = lax.all_to_all(sent, SP, 0, 0, tiled=True).reshape(2 * slots, half)]
    all_to_all x1, waiting for transfers between devices: 35.7 us -> 8.24 us  [on_device(): lax.all_to_all(jnp.stack([lax.dot_general(slot_tokens, flat_rows, (((0,),...]
    all_gather x1 -> x0, blocking collectives: 16.1 us -> none  [on_device(): lax.all_gather(lax.dot_general(slot_tokens, flat_rows, (((0,), (0,)), (()...]
    all_to_all x3, waiting for transfers between devices: 19.1 us -> 34.8 us  [to_all(): return lax.all_to_all(copies, axis, 0, 0, tiled=True)]
    all_to_all x1, starting transfers between devices: 13.6 us -> 3.57 us  [on_device(): lax.all_to_all(jnp.stack([lax.dot_general(slot_tokens, flat_rows, (((0,),...]
    all_to_all x1, waiting for transfers between devices: 14.4 us -> 22.8 us  [on_device(): lax.all_to_all(parts, 'y', 0, 0, tiled=True)]
    all_to_all x1, waiting for transfers between devices: 20.1 us -> 24 us  [on_device(): lax.all_to_all(share.reshape(sp_count, model_width // sp_count, -1), SP,...]
  transfers between devices with their start and end apart: 9 -> 9, of which waited for: 8 -> 8; matrix products, arithmetic and copies ran while one was open for 15% -> 14% of each run, Pallas kernels for 0% -> 0%
where the time goes in v1:
time: 254 us; the launch traced here: 252 us
  waiting for transfers between devices  98.9 us (39%)
  blocking collectives  52.7 us (21%)
  starting transfers between devices  40.7 us (16%)
  other arithmetic  30.1 us (12%)
  local copies, waits for them, and re-layouts  14.2 us (6%)
  matrix products  13.8 us (5%)
    all_to_all x1, blocking collectives, on_device(): own = lax.all_to_all(sent, SP, 0, 0, tiled=True).reshape(2 * slots, half)  52.7 us
    all_to_all x3, waiting for transfers between devices, to_all(): return lax.all_to_all(copies, axis, 0, 0, tiled=True)  34.8 us
    all_to_all x1, waiting for transfers between devices, on_device(): lax.all_to_all(share.reshape(sp_count, model_width // sp_count, -1), SP,...  24 us
    all_to_all x1, waiting for transfers between devices, on_device(): lax.all_to_all(parts, 'y', 0, 0, tiled=True)  22.8 us
    all_to_all x3, starting transfers between devices, to_all(): return lax.all_to_all(copies, axis, 0, 0, tiled=True)  15.2 us
    all_to_all x1, waiting for transfers between devices, on_device(): lax.all_to_all(summed.reshape(experts, capacity, -1), SP, split_axis=0, c...  8.42 us
    all_to_all x1, waiting for transfers between devices, on_device(): lax.all_to_all(jnp.stack([lax.dot_general(slot_tokens, flat_rows, (((0,),...  8.24 us
    all_to_all x1, starting transfers between devices, on_device(): lax.all_to_all(parts, 'y', 0, 0, tiled=True)  7.09 us
  transfers between devices with their start and end apart: 9, of which 8 were waited for; matrix products, arithmetic and copies ran while one was open for 14% of the time, Pallas kernels for 0%

profile of v1, /device:TPU:2, one launch (start us, length us, event | category | flops | bytes accessed | tf_op | source)
XLA Modules:
  0.0 252.2 jit_solution(4890277538563998212)
XLA Ops:
  0.7 0.8 copy.116
  1.8 0.8 slice_bitcast_fusion.11
  3.7 0.7 multiply_add_fusion
  4.4 1.3 copy.121
  7.7 52.7 %all_to_all.40 = bf16[32,24,1024]{2,1,0:T(8,128)(2,1)S(1)} all-to-all(bf16[32,24,1024]{2,1,0:T(8,128)(2,1)S(1)} %bitcast.390), channel_id=1, replica_groups=mesh['z'=8,'x'=4,'y'=8,'c'=2] {'z','x'}, dimensions={0} | all-to-all | bytes 3145728 | tf_op jit(solution)/shard_map/all_to_all | solution.py:168
  60.4 1.9 collective-permute-start
  62.8 1.9 broadcast_select_fusion.4
  64.6 1.1 fusion.149
  66.1 1.0 fusion.23
  67.3 2.0 fusion.45
  69.4 0.9 select_convert_fusion
  71.4 2.3 collective-permute-start.1
  76.1 1.1 copy.154
  77.2 7.1 %all-to-all-start.1 = ((bf16[8,384,128]{2,1,0:T(8,128)(2,1)}), bf16[8,384,128]{2,1,0:T(8,128)(2,1)}, u32[]{:S(2)}, u32[]{:S(2)}) async-start(bf16[8,384,128]{2,1,0:T(8,128)(2,1)} %bitcast.381), calls=%async_computation.1 | async-start | bytes 1572864 | tf_op jit(solution)/shard_map/all_to_all | solution.py:210
  85.2 22.8 %all-to-all-done.1 = bf16[8,384,128]{2,1,0:T(8,128)(2,1)} async-done(((bf16[8,384,128]{2,1,0:T(8,128)(2,1)}), bf16[8,384,128]{2,1,0:T(8,128)(2,1)}, u32[]{:S(2)}, u32[]{:S(2)}) %all-to-all-start.1) | async-done | bytes 786464 | tf_op jit(solution)/shard_map/all_to_all | solution.py:210
  108.0 1.2 reduce_sum.81
  109.3 0.7 reshape.967
  110.0 5.6 %all-to-all-start.2 = ((bf16[32,12,128]{2,1,0:T(8,128)(2,1)}), bf16[32,12,128]{2,1,0:T(8,128)(2,1)S(1)}, u32[]{:S(2)}, u32[]{:S(2)}) async-start(bf16[32,12,128]{2,1,0:T(8,128)(2,1)} %reshape.967), calls=%async_computation.2 | async-start | bytes 262144 | tf_op jit(solution)/shard_map/all_to_all | solution.py:231
  116.1 8.4 %all-to-all-done.2 = bf16[32,12,128]{2,1,0:T(8,128)(2,1)S(1)} async-done(((bf16[32,12,128]{2,1,0:T(8,128)(2,1)}), bf16[32,12,128]{2,1,0:T(8,128)(2,1)S(1)}, u32[]{:S(2)}, u32[]{:S(2)}) %all-to-all-start.2) | async-done | bytes 98336 | tf_op jit(solution)/shard_map/all_to_all | solution.py:231
  124.8 0.9 stack.2
  125.7 3.6 %all-to-all-start.3 = ((bf16[16,128,128]{2,1,0:T(8,128)(2,1)}), bf16[16,128,128]{2,1,0:T(8,128)(2,1)S(1)}, u32[]{:S(2)}, u32[]{:S(2)}) async-start(bf16[16,128,128]{2,1,0:T(8,128)(2,1)} %stack.2), calls=%async_computation.3 | async-start | bytes 1048576 | tf_op jit(solution)/shard_map/all_to_all | solution.py:240
  129.4 5.4 %fusion.4 = (bf16[2,64,64]{2,1,0:T(8,128)(2,1)}, f32[2,64,128,64]{2,3,1,0:T(8,128)}) fusion(f32[2,128,64]{1,2,0:T(8,128)} %get-tuple-element.306, f32[2,128,64]{1,2,0:T(8,128)} %bitcast.391, f32[2,64,128]{2,1,0:T(8,128)S(1)} %bitcast.379, pred[64,64]{1,0:T(8,128)(4,1)S(1)} %iota_compare_fusion.10), kind=kLoop, calls=%fused_computation.11 | loop fusion | flops 5234688 | bytes 4411392 | tf_op jit(solution)/shard_map/vmap(ntd,nsd,ntsd->nts)/dot_general | solution.py:91
  134.9 1.0 convolution_convert_fusion.1
  135.9 1.1 fusion.147
  137.0 8.2 %all-to-all-done.3 = bf16[16,128,128]{2,1,0:T(8,128)(2,1)S(1)} async-done(((bf16[16,128,128]{2,1,0:T(8,128)(2,1)}), bf16[16,128,128]{2,1,0:T(8,128)(2,1)S(1)}, u32[]{:S(2)}, u32[]{:S(2)}) %all-to-all-start.3) | async-done | bytes 524320 | tf_op jit(solution)/shard_map/all_to_all | solution.py:240
  145.2 1.9 broadcast_in_dim.169
  147.1 6.2 %all-to-all-start.5 = ((bf16[32,64,256]{2,1,0:T(8,128)(2,1)}), bf16[32,64,256]{2,1,0:T(8,128)(2,1)}, u32[]{:S(2)}, u32[]{:S(2)}) async-start(bf16[32,64,256]{2,1,0:T(8,128)(2,1)} %broadcast_in_dim.169), calls=%async_computation.5 | async-start | bytes 2097152 | tf_op jit(solution)/shard_map/all_to_all | solution.py:34
  153.3 1.9 maximum_bitcast_fusion
  155.2 0.7 slice.339
  155.9 1.9 maximum_bitcast_fusion.1
  157.7 2.0 convolution_convert_fusion.3
  159.8 0.8 maximum_bitcast_fusion.2
  161.8 20.1 %all-to-all-done.5 = bf16[32,64,256]{2,1,0:T(8,128)(2,1)} async-done(((bf16[32,64,256]{2,1,0:T(8,128)(2,1)}), bf16[32,64,256]{2,1,0:T(8,128)(2,1)}, u32[]{:S(2)}, u32[]{:S(2)}) %all-to-all-start.5) | async-done | bytes 1048608 | tf_op jit(solution)/shard_map/all_to_all | solution.py:34
  181.8 1.6 convolution_convert_fusion.4
  184.4 0.7 broadcast_in_dim.173
  185.1 5.5 %all-to-all-start.6 = ((bf16[4,136,256]{2,1,0:T(8,128)(2,1)}), bf16[4,136,256]{2,1,0:T(8,128)(2,1)S(1)}, u32[]{:S(2)}, u32[]{:S(2)}) async-start(bf16[4,136,256]{2,1,0:T(8,128)(2,1)} %broadcast_in_dim.173), calls=%async_computation.6 | async-start | bytes 557056 | tf_op jit(solution)/shard_map/all_to_all | solution.py:34
  190.9 5.6 %all-to-all-done.6 = bf16[4,136,256]{2,1,0:T(8,128)(2,1)S(1)} async-done(((bf16[4,136,256]{2,1,0:T(8,128)(2,1)}), bf16[4,136,256]{2,1,0:T(8,128)(2,1)S(1)}, u32[]{:S(2)}, u32[]{:S(2)}) %all-to-all-start.6) | async-done | bytes 278560 | tf_op jit(solution)/shard_map/all_to_all | solution.py:34
  196.7 0.9 broadcast_in_dim.175
  197.5 3.5 %all-to-all-start.7 = ((bf16[8,136,256]{2,1,0:T(8,128)(2,1)}), bf16[8,136,256]{2,1,0:T(8,128)(2,1)S(1)}, u32[]{:S(2)}, u32[]{:S(2)}) async-start(bf16[8,136,256]{2,1,0:T(8,128)(2,1)} %broadcast_in_dim.175), calls=%async_computation.7 | async-start | bytes 1114112 | tf_op jit(solution)/shard_map/all_to_all | solution.py:34
  201.1 5.0 %fusion.5 = f32[2,64,128]{2,1,0:T(8,128)S(1)} fusion(f32[2,64,128,64]{2,3,1,0:T(8,128)} %get-tuple-element.299, f32[2,64,128]{2,1,0:T(8,128)S(1)} %copy-done.14, f32[2,64,64]{2,1,0:T(8,128)S(1)} %copy.127), kind=kLoop, calls=%fused_computation.13 | loop fusion | flops 3129344 | bytes 4358144 | tf_op jit(solution)/shard_map/vmap(nts,nsd,ntsd->ntd)/dot_general | solution.py:94
  206.2 1.4 convolution_convert_fusion
  207.7 1.9 multiply_reduce_fusion
  209.7 9.1 %all-to-all-done.7 = bf16[8,136,256]{2,1,0:T(8,128)(2,1)S(1)} async-done(((bf16[8,136,256]{2,1,0:T(8,128)(2,1)}), bf16[8,136,256]{2,1,0:T(8,128)(2,1)S(1)}, u32[]{:S(2)}, u32[]{:S(2)}) %all-to-all-start.7) | async-done | bytes 557088 | tf_op jit(solution)/shard_map/all_to_all | solution.py:34
  218.8 5.0 %all-to-all-start.4 = ((bf16[32,64,256]{2,1,0:T(8,128)(2,1)}), bf16[32,64,256]{2,1,0:T(8,128)(2,1)S(1)}, u32[]{:S(2)}, u32[]{:S(2)}) async-start(bf16[32,64,256]{2,1,0:T(8,128)(2,1)} %bitcast.30), calls=%async_computation.4 | async-start | bytes 2097152 | tf_op jit(solution)/shard_map/all_to_all | solution.py:270
  224.2 0.9 multiply_subtract_fusion
  226.5 0.8 fusion.12
  227.4 24.0 %all-to-all-done.4 = bf16[32,64,256]{2,1,0:T(8,128)(2,1)S(1)} async-done(((bf16[32,64,256]{2,1,0:T(8,128)(2,1)}), bf16[32,64,256]{2,1,0:T(8,128)(2,1)S(1)}, u32[]{:S(2)}, u32[]{:S(2)}) %all-to-all-start.4) | async-done | bytes 1048608 | tf_op jit(solution)/shard_map/all_to_all | solution.py:270
  251.4 0.8 convert_reduce_fusion
  (161 shorter events, 14.3 us)
Async XLA Ops:
  0.6 205.6 %copy-start = (bf16[128,256]{1,0:T(8,128)(2,1)S(1)}, bf16[128,256]{1,0:T(8,128)(2,1)}, u32[]{:S(2)}) copy-start(bf16[128,256]{1,0:T(8,128)(2,1)} %param.28) | copy-start | bytes 196612
  0.6 5.1 %copy-start.11 = (bf16[128,2048]{1,0:T(8,128)(2,1)S(1)}, bf16[128,2048]{1,0:T(8,128)(2,1)}, u32[]{:S(2)}) copy-start(bf16[128,2048]{1,0:T(8,128)(2,1)} %param.19) | copy-start | bytes 1572868
  1.5 5.1 %copy-start.23 = (f32[2048]{0:T(1024)S(1)}, f32[2048]{0:T(1024)}, u32[]{:S(2)}) copy-start(f32[2048]{0:T(1024)} %param.20) | copy-start | bytes 24580
  6.3 1.3 copy-start.28
  7.6 54.7 %copy-start.24 = (f32[128,128]{1,0:T(8,128)S(1)}, f32[128,128]{1,0:T(8,128)}, u32[]{:S(2)}) copy-start(f32[128,128]{1,0:T(8,128)} %param.32) | copy-start | bytes 196612
  7.6 54.8 %copy-start.7 = (bf16[128,256]{1,0:T(8,128)(2,1)S(1)}, bf16[128,256]{1,0:T(8,128)(2,1)}, u32[]{:S(2)}) copy-start(bf16[128,256]{1,0:T(8,128)(2,1)} %param.31) | copy-start | bytes 196612
  7.7 54.8 %copy-start.12 = (bf16[128,128]{1,0:T(8,128)(2,1)S(1)}, bf16[128,128]{1,0:T(8,128)(2,1)}, u32[]{:S(2)}) copy-start(bf16[128,128]{1,0:T(8,128)(2,1)} %param.30) | copy-start | bytes 98308
  60.4 5.5 %collective-permute-start = (bf16[768,1024]{1,0:T(8,128)(2,1)S(1)}, bf16[768,1024]{1,0:T(8,128)(2,1)}, u32[]{:S(2)}, u32[]{:S(2)}) collective-permute-start(bf16[768,1024]{1,0:T(8,128)(2,1)S(1)} %bitcast.376), channel_id=1, source_target_pairs={{0,1},{1,0},{2,3},{3,2},{4,5},{5,4},{6,7},{7,6},{8,9},{9,8},{10,11... | collective-permute-start | bytes 4718600 | tf_op jit(solution)/shard_map/ppermute | solution.py:169
  62.4 3.3 %copy-start.25 = (f32[1,2,1,128]{3,2,1,0:T(1,128)}, f32[1,2,1,128]{3,2,1,0:T(1,128)S(1)}, u32[]{:S(2)}) copy-start(f32[1,2,1,128]{3,2,1,0:T(1,128)S(1)} %get-tuple-element.305) | copy-start | bytes 3076
  62.7 3.0 %copy-start.2 = (bf16[1,2048,128]{2,1,0:T(8,128)(2,1)S(1)}, bf16[1,2048,128]{2,1,0:T(8,128)(2,1)}, u32[]{:S(2)}) copy-start(bf16[1,2048,128]{2,1,0:T(8,128)(2,1)} %param.25) | copy-start | bytes 1572868
  62.7 3.0 %copy-start.3 = (bf16[1,2048,128]{2,1,0:T(8,128)(2,1)S(1)}, bf16[1,2048,128]{2,1,0:T(8,128)(2,1)}, u32[]{:S(2)}) copy-start(bf16[1,2048,128]{2,1,0:T(8,128)(2,1)} %param.24) | copy-start | bytes 1572868
  66.1 1.1 copy-start.4
  70.6 5.4 %copy-start.16 = (bf16[768,128]{1,0:T(8,128)(2,1)}, bf16[768,128]{1,0:T(8,128)(2,1)S(1)}, u32[]{:S(2)}) copy-start(bf16[768,128]{1,0:T(8,128)(2,1)S(1)} %get-tuple-element.276) | copy-start | bytes 589828
  70.6 5.4 %copy-start.18 = (bf16[768,128]{1,0:T(8,128)(2,1)}, bf16[768,128]{1,0:T(8,128)(2,1)S(1)}, u32[]{:S(2)}) copy-start(bf16[768,128]{1,0:T(8,128)(2,1)S(1)} %get-tuple-element.277) | copy-start | bytes 589828
  70.6 3.7 %copy-start.21 = (bf16[128,128]{1,0:T(8,128)(2,1)S(1)}, bf16[128,128]{1,0:T(8,128)(2,1)}, u32[]{:S(2)}) copy-start(bf16[128,128]{1,0:T(8,128)(2,1)} %param.29) | copy-start | bytes 98308
  71.4 4.2 %collective-permute-start.1 = (bf16[384,1024]{1,0:T(8,128)(2,1)S(1)}, bf16[384,1024]{1,0:T(8,128)(2,1)S(1)}, u32[]{:S(2)}, u32[]{:S(2)}) collective-permute-start(bf16[384,1024]{1,0:T(8,128)(2,1)S(1)} %convolution_convert_fusion.2), channel_id=1, source_target_pairs={{0,1},{1,0},{2,3},{3,2},{4,5},{5,4},{6,7},{7,6},{8,9},{9,8},{10,11... | collective-permute-start | bytes 2359304 | tf_op jit(solution)/shard_map/ppermute | solution.py:207
  76.1 8.9 %copy-start.1 = (f32[1,1,128,256]{3,2,1,0:T(8,128)S(1)}, f32[1,1,128,256]{3,2,1,0:T(8,128)}, u32[]{:S(2)}) copy-start(f32[1,1,128,256]{3,2,1,0:T(8,128)} %param.33) | copy-start | bytes 393220
  77.2 30.9 %all-to-all-start.1 = ((bf16[8,384,128]{2,1,0:T(8,128)(2,1)}), bf16[8,384,128]{2,1,0:T(8,128)(2,1)}, u32[]{:S(2)}, u32[]{:S(2)}) async-start(bf16[8,384,128]{2,1,0:T(8,128)(2,1)} %bitcast.381), calls=%async_computation.1 | async-start | bytes 1572864 | tf_op jit(solution)/shard_map/all_to_all | solution.py:210
  85.2 40.5 %copy-start.9 = (bf16[2,1,128,256]{3,2,1,0:T(8,128)(2,1)}, bf16[2,1,128,256]{3,2,1,0:T(8,128)(2,1)S(1)}, u32[]{:S(2)}) copy-start(bf16[2,1,128,256]{3,2,1,0:T(8,128)(2,1)S(1)} %get-tuple-element.142) | copy-start | bytes 393220
  85.2 40.5 %copy-start.30 = (f32[2,1,128]{2,1,0:T(1,128)}, f32[2,1,128]{2,1,0:T(1,128)S(1)}, u32[]{:S(2)}) copy-start(f32[2,1,128]{2,1,0:T(1,128)S(1)} %get-tuple-element.450) | copy-start | bytes 3076
  110.0 14.6 %all-to-all-start.2 = ((bf16[32,12,128]{2,1,0:T(8,128)(2,1)}), bf16[32,12,128]{2,1,0:T(8,128)(2,1)S(1)}, u32[]{:S(2)}, u32[]{:S(2)}) async-start(bf16[32,12,128]{2,1,0:T(8,128)(2,1)} %reshape.967), calls=%async_computation.2 | async-start | bytes 262144 | tf_op jit(solution)/shard_map/all_to_all | solution.py:231
  125.7 19.5 %all-to-all-start.3 = ((bf16[16,128,128]{2,1,0:T(8,128)(2,1)}), bf16[16,128,128]{2,1,0:T(8,128)(2,1)S(1)}, u32[]{:S(2)}, u32[]{:S(2)}) async-start(bf16[16,128,128]{2,1,0:T(8,128)(2,1)} %stack.2), calls=%async_computation.3 | async-start | bytes 1048576 | tf_op jit(solution)/shard_map/all_to_all | solution.py:240
  129.4 5.5 %copy-start.19 = (bf16[768,128]{1,0:T(8,128)(2,1)S(1)}, bf16[768,128]{1,0:T(8,128)(2,1)}, u32[]{:S(2)}) copy-start(bf16[768,128]{1,0:T(8,128)(2,1)} %copy-done.18) | copy-start | bytes 589828
  129.4 5.5 %copy-start.17 = (bf16[768,128]{1,0:T(8,128)(2,1)S(1)}, bf16[768,128]{1,0:T(8,128)(2,1)}, u32[]{:S(2)}) copy-start(bf16[768,128]{1,0:T(8,128)(2,1)} %copy-done.16) | copy-start | bytes 589828
  129.4 5.5 %copy-start.5 = (bf16[768,1024]{1,0:T(8,128)(2,1)S(1)}, bf16[768,1024]{1,0:T(8,128)(2,1)}, u32[]{:S(2)}) copy-start(bf16[768,1024]{1,0:T(8,128)(2,1)} %copy-done.4) | copy-start | bytes 4718596
  147.1 34.7 %all-to-all-start.5 = ((bf16[32,64,256]{2,1,0:T(8,128)(2,1)}), bf16[32,64,256]{2,1,0:T(8,128)(2,1)}, u32[]{:S(2)}, u32[]{:S(2)}) async-start(bf16[32,64,256]{2,1,0:T(8,128)(2,1)} %broadcast_in_dim.169), calls=%async_computation.5 | async-start | bytes 2097152 | tf_op jit(solution)/shard_map/all_to_all | solution.py:34
  153.3 4.4 %copy-start.15 = (bf16[768,128]{1,0:T(8,128)(2,1)S(1)}, bf16[768,128]{1,0:T(8,128)(2,1)}, u32[]{:S(2)}) copy-start(bf16[768,128]{1,0:T(8,128)(2,1)} %get-tuple-element.274) | copy-start | bytes 589828
  159.8 1.2 copy-start.29
  161.3 22.1 %copy-start.6 = (f32[128,128]{1,0:T(8,128)S(1)}, f32[128,128]{1,0:T(8,128)}, u32[]{:S(2)}) copy-start(f32[128,128]{1,0:T(8,128)} %convert_multiply_fusion.17) | copy-start | bytes 196612
  161.8 21.9 %copy-start.31 = (f32[2,1,128]{2,1,0:T(1,128)S(1)}, f32[2,1,128]{2,1,0:T(1,128)}, u32[]{:S(2)}) copy-start(f32[2,1,128]{2,1,0:T(1,128)} %copy-done.30) | copy-start | bytes 3076
  183.7 0.7 copy-start.32
  183.7 6.9 %copy-start.8 = (bf16[128,256]{1,0:T(8,128)(2,1)S(1)}, bf16[128,256]{1,0:T(8,128)(2,1)}, u32[]{:S(2)}) copy-start(bf16[128,256]{1,0:T(8,128)(2,1)} %param.31) | copy-start | bytes 196612
  185.1 15.9 %copy-start.14 = (f32[2,64,128]{2,1,0:T(8,128)S(1)}, f32[2,64,128]{2,1,0:T(8,128)}, u32[]{:S(2)}) copy-start(f32[2,64,128]{2,1,0:T(8,128)} %get-tuple-element.307) | copy-start | bytes 196612
  185.1 11.4 %all-to-all-start.6 = ((bf16[4,136,256]{2,1,0:T(8,128)(2,1)}), bf16[4,136,256]{2,1,0:T(8,128)(2,1)S(1)}, u32[]{:S(2)}, u32[]{:S(2)}) async-start(bf16[4,136,256]{2,1,0:T(8,128)(2,1)} %broadcast_in_dim.173), calls=%async_computation.6 | async-start | bytes 557056 | tf_op jit(solution)/shard_map/all_to_all | solution.py:34
  197.5 21.3 %all-to-all-start.7 = ((bf16[8,136,256]{2,1,0:T(8,128)(2,1)}), bf16[8,136,256]{2,1,0:T(8,128)(2,1)S(1)}, u32[]{:S(2)}, u32[]{:S(2)}) async-start(bf16[8,136,256]{2,1,0:T(8,128)(2,1)} %broadcast_in_dim.175), calls=%async_computation.7 | async-start | bytes 1114112 | tf_op jit(solution)/shard_map/all_to_all | solution.py:34
  201.1 5.0 %copy-start.10 = (bf16[2,1,128,256]{3,2,1,0:T(8,128)(2,1)S(1)}, bf16[2,1,128,256]{3,2,1,0:T(8,128)(2,1)}, u32[]{:S(2)}) copy-start(bf16[2,1,128,256]{3,2,1,0:T(8,128)(2,1)} %copy-done.9) | copy-start | bytes 393220
  209.6 14.6 %copy-start.13 = (bf16[128,128]{1,0:T(8,128)(2,1)S(1)}, bf16[128,128]{1,0:T(8,128)(2,1)}, u32[]{:S(2)}) copy-start(bf16[128,128]{1,0:T(8,128)(2,1)} %param.30) | copy-start | bytes 98308
  209.6 14.6 %copy-start.22 = (bf16[128,128]{1,0:T(8,128)(2,1)S(1)}, bf16[128,128]{1,0:T(8,128)(2,1)}, u32[]{:S(2)}) copy-start(bf16[128,128]{1,0:T(8,128)(2,1)} %param.29) | copy-start | bytes 98308
  209.7 14.6 %copy-start.26 = (f32[1,2,1,128]{3,2,1,0:T(1,128)S(1)}, f32[1,2,1,128]{3,2,1,0:T(1,128)}, u32[]{:S(2)}) copy-start(f32[1,2,1,128]{3,2,1,0:T(1,128)} %copy-done.25) | copy-start | bytes 3076
  209.7 14.6 %copy-start.27 = (f32[2,128]{1,0:T(2,128)S(1)}, f32[2,128]{1,0:T(2,128)}, u32[]{:S(2)}) copy-start(f32[2,128]{1,0:T(2,128)} %subtract_exponential_fusion.1) | copy-start | bytes 3076
  218.8 32.6 %all-to-all-start.4 = ((bf16[32,64,256]{2,1,0:T(8,128)(2,1)}), bf16[32,64,256]{2,1,0:T(8,128)(2,1)S(1)}, u32[]{:S(2)}, u32[]{:S(2)}) async-start(bf16[32,64,256]{2,1,0:T(8,128)(2,1)} %bitcast.30), calls=%async_computation.4 | async-start | bytes 2097152 | tf_op jit(solution)/shard_map/all_to_all | solution.py:270
  224.2 2.3 copy-start.20
